TPU v7x, 32 devices: a whole 2x2x4 slice. The times are simulated.
32 devices in a mesh: fs: 8 (over z, core), tp: 4 (over y, x).
Axes of the slice: x: 2, y: 2, z: 4, core: 2. Of those that a mesh axis runs over, the one named last changes fastest.
Arguments:
- tokens: bfloat16 [4096, 4096], P('fs', 'tp'), may hold values from -16 to 16
- norm_gain: float32 [4096], P('fs'), may hold values from 0.1 to 1.9
- gate_train: float32 [4096, 12288], P('fs', 'tp'), may hold values from -6 to 6
- up_train: float32 [4096, 12288], P('fs', 'tp'), may hold values from -6 to 6
Outputs:
- gate_serve: bfloat16 [4096, 12288], P(None, 'tp')
- up_serve: bfloat16 [4096, 12288], P(None, 'tp')
- hidden: bfloat16 [4096, 12288], P('fs', 'tp')
All inputs are finite; a program needn't handle non-finite values.
Results may differ from a plain program's by a relative error of at most 0.0071.
Values may be sent and summed in bfloat16 or wider, within the bound.
A program may use at most 192 MiB of HBM per device.

v0:
```python
import jax
import jax.numpy as jnp
from jax import lax
from jax.sharding import PartitionSpec as P


def body(tokens, norm_gain, gate_train, up_train):
    gain = norm_gain[:, None]
    gate_local = (gate_train * gain).astype(jnp.bfloat16)
    up_local = (up_train * gain).astype(jnp.bfloat16)
    whole = lax.all_gather(tokens, "tp", axis=1, tiled=True)
    values = whole.astype(jnp.float32)
    normed = (values * lax.rsqrt(jnp.mean(values * values, axis=-1, keepdims=True) + 1e-06)).astype(
        jnp.bfloat16
    )
    width = normed.shape[1]
    scale = width ** (-0.5)
    gate_serve, up_serve = (
        lax.all_gather(gate_local, "fs", axis=0, tiled=True),
        lax.all_gather(up_local, "fs", axis=0, tiled=True),
    )
    gate_acc = jnp.dot(normed, gate_serve, preferred_element_type=jnp.float32)
    up_acc = jnp.dot(normed, up_serve, preferred_element_type=jnp.float32)
    gate = gate_acc * scale
    up = up_acc * scale
    hidden = (jax.nn.silu(gate) * up).astype(jnp.bfloat16)
    return (gate_serve, up_serve, hidden)


def solution(mesh):
    in_specs = (P("fs", "tp"), P("fs"), P("fs", "tp"), P("fs", "tp"))
    out_specs = (P(None, "tp"), P(None, "tp"), P("fs", "tp"))
    return jax.shard_map(body, mesh=mesh, in_specs=in_specs, out_specs=out_specs, check_vma=False)
```

profile of v0, /device:TPU:0, one launch (start us, length us, event | category | flops | bytes accessed | tf_op | source)
XLA Modules:
  0.0 569.7 jit_solution(12411793271498854987)
XLA Ops:
  7.2 0.0 all-gather.8.cloned.1.call-start
  7.2 0.7 all-gather.8.cloned.1.call-update
  7.9 0.0 all-gather.4.cloned.1.call-start
  7.9 9.3 %multiply_convert_fusion.1 = (bf16[512,3072]{1,0:T(8,128)(2,1)}, bf16[512,3072]{1,0:T(8,128)(2,1)}) fusion(f32[512,3072]{1,0:T(8,128)} %param.7, f32[512]{0:T(512)} %param.5, f32[512,3072]{1,0:T(8,128)} %param.6), kind=kLoop, calls=%fused_computation.5 | loop fusion | flops 6291456 | bytes 18876416 | tf_op jit(solution)/shard_map/convert_element_type | solution.py:10
  17.2 0.0 all-gather.4.cloned.1.call-update
  17.3 0.0 all-gather.6.cloned.1.call-start
  17.3 0.7 all-gather.6.cloned.1.call-update
  18.0 47.2 %all-gather.8.cloned.1.call-done = bf16[512,4096]{1,0:T(8,128)(2,1)} async-done(((bf16[512,1024]{1,0:T(8,128)(2,1)}), bf16[512,4096]{1,0:T(8,128)(2,1)}) %all-gather.8.cloned.1.call-update) | async-done | bytes 4194320 | tf_op jit(solution)/shard_map/all_gather | solution.py:11
  65.1 3.1 fusion
  68.2 219.0 %all-gather.4.cloned.1.call-done = bf16[4096,3072]{1,0:T(8,128)(2,1)} async-done(((bf16[512,3072]{1,0:T(8,128)(2,1)}), bf16[4096,3072]{1,0:T(8,128)(2,1)}) %all-gather.4.cloned.1.call-update) | async-done | bytes 25165840 | tf_op jit(solution)/shard_map/all_gather | solution.py:19
  287.2 20.6 %fusion.3 = f32[512,3072]{1,0:T(8,128)} fusion(bf16[4096,3072]{1,0:T(8,128)(2,1)} %all-gather.4.cloned.1.call-done, bf16[512,4096]{1,0:T(8,128)(2,1)} %all-gather.8.cloned.1.call-done, f32[512]{0:T(512)S(1)} %add_rsqrt_fusion), kind=kOutput, calls=%fused_computation.7 | convolution fusion | flops 12891193344 | bytes 35653632 | tf_op jit(solution)/shard_map/dot_general | solution.py:22
  307.8 199.7 %all-gather.6.cloned.1.call-done = bf16[4096,3072]{1,0:T(8,128)(2,1)} async-done(((bf16[512,3072]{1,0:T(8,128)(2,1)}), bf16[4096,3072]{1,0:T(8,128)(2,1)}) %all-gather.6.cloned.1.call-update) | async-done | bytes 25165840 | tf_op jit(solution)/shard_map/all_gather | solution.py:20
  507.5 21.8 %multiply_convert_fusion = bf16[512,3072]{1,0:T(8,128)(2,1)} fusion(f32[512,3072]{1,0:T(8,128)} %fusion.3, bf16[4096,3072]{1,0:T(8,128)(2,1)} %all-gather.6.cloned.1.call-done, bf16[512,4096]{1,0:T(8,128)(2,1)} %all-gather.8.cloned.1.call-done, f32[512]{0:T(512)S(1)} %add_rsqrt_fusion), kind=kOutput, calls=%fused_computation.4 | convolution fusion | flops 12903776256 | bytes 38799360 | tf_op jit(solution)/shard_map/dot_general | solution.py:23
  529.4 0.0 copy-start
  529.4 22.0 %copy.9 = bf16[4096,3072]{1,0:T(8,128)(2,1)} copy(bf16[4096,3072]{1,0:T(8,128)(2,1)} %all-gather.4.cloned.1.call-done) | data formatting | bytes 50331648
  551.3 2.9 copy-done
  554.3 8.9 %copy.10 = bf16[4096,3072]{1,0:T(8,128)(2,1)} copy(bf16[4096,3072]{1,0:T(8,128)(2,1)S(1)} %copy-done) | data formatting | bytes 50331648
  (1 shorter events, 0.0 us)
Async XLA Ops:
  7.2 58.0 %all-gather.8.cloned.1.call-start = ((), (), s32[]{:S(2)}) async-start(), calls=%async_computation.2 | async-start | bytes 5242880 | tf_op jit(solution)/shard_map/all_gather | solution.py:11
  7.9 279.3 %all-gather.4.cloned.1.call-start = ((), (), s32[]{:S(2)}) async-start(), calls=%async_computation | async-start | bytes 28311552 | tf_op jit(solution)/shard_map/all_gather | solution.py:19
  17.3 490.3 %all-gather.6.cloned.1.call-start = ((), (), s32[]{:S(2)}) async-start(), calls=%async_computation.1 | async-start | bytes 28311552 | tf_op jit(solution)/shard_map/all_gather | solution.py:20
  529.4 24.9 %copy-start = (bf16[4096,3072]{1,0:T(8,128)(2,1)S(1)}, bf16[4096,3072]{1,0:T(8,128)(2,1)}, u32[]{:S(2)}) copy-start(bf16[4096,3072]{1,0:T(8,128)(2,1)} %all-gather.6.cloned.1.call-done) | copy-start | bytes 75497472
Sparse Core Ops, SparseCore 0:
  9.8 55.2 all-gather.7
  67.4 219.8 all-gather.3
  289.5 218.0 all-gather.5
where the time goes:
time: 570 us
  waiting for transfers between devices  467 us (82%)
  matrix products  42.4 us (7%)
  local copies, waits for them, and re-layouts  33.8 us (6%)
  between operations  13.7 us (2%)
  other arithmetic  12.4 us (2%)
    all_gather x1, waiting for transfers between devices, body(): lax.all_gather(gate_local, 'fs', axis=0, tiled=True)  219 us
    all_gather x1, waiting for transfers between devices, body(): lax.all_gather(up_local, 'fs', axis=0, tiled=True)  200 us
    all_gather x1, waiting for transfers between devices, body(): whole = lax.all_gather(tokens, 'tp', axis=1, tiled=True)  47.2 us
    unnamed x4, local copies, waits for them, and re-layouts  33.8 us
    dot_general x1, matrix products, body(): up_acc = jnp.dot(normed, up_serve, preferred_element_type=jnp.float32)  21.8 us
    dot_general x1, matrix products, body(): gate_acc = jnp.dot(normed, gate_serve, preferred_element_type=jnp.float32)  20.6 us
  transfers between devices with their start and end apart: 3, of which 3 were waited for; matrix products, arithmetic and copies ran while one was open for 6% of the time, Pallas kernels for 0%

commit v1 on v0

--- a/solution.py
+++ b/solution.py
@@ -4,11 +4,27 @@
 from jax.sharding import PartitionSpec as P
 
 
+def find_thing_all(z_in):
+    n_peers_all = lax.axis_size("tp")
+    sheets = [(i0, (i0 + 1) % n_peers_all) for i0 in range(n_peers_all)]
+
+    def plan_islands(seen_now):
+        if len(seen_now) == n_peers_all:
+            return seen_now
+        prior = plan_islands([lax.ppermute(seen_now[0], "tp", sheets), *seen_now])
+        return prior
+
+    built = plan_islands([z_in])
+    f_next = jnp.concatenate(built, 1)
+    frame_out = jnp.roll(f_next, (lax.axis_index("tp") + 1) * z_in.shape[1], 1)
+    return frame_out
+
+
 def body(tokens, norm_gain, gate_train, up_train):
     gain = norm_gain[:, None]
     gate_local = (gate_train * gain).astype(jnp.bfloat16)
     up_local = (up_train * gain).astype(jnp.bfloat16)
-    whole = lax.all_gather(tokens, "tp", axis=1, tiled=True)
+    whole = find_thing_all(tokens)
     values = whole.astype(jnp.float32)
     normed = (values * lax.rsqrt(jnp.mean(values * values, axis=-1, keepdims=True) + 1e-06)).astype(
         jnp.bfloat16

time: 570 us -> 522 us (0.916)
  waiting for transfers between devices: 467 us -> 411 us
  local copies, waits for them, and re-layouts: 33.8 us -> 40.4 us
    all_gather x1, waiting for transfers between devices: 219 us -> 137 us  [body(): lax.all_gather(gate_local, 'fs', axis=0, tiled=True)]
    ppermute x0 -> x3, waiting for transfers between devices: none -> 73.3 us  [plan_islands(): prior = plan_islands([lax.ppermute(seen_now[0], 'tp', sheets), *seen_now])]
    all_gather x1 -> x0, waiting for transfers between devices: 47.2 us -> none  [body(): whole = lax.all_gather(tokens, 'tp', axis=1, tiled=True)]
    unnamed x4 -> x15, local copies, waits for them, and re-layouts: 33.8 us -> 40.3 us
  transfers between devices with their start and end apart: 3 -> 5, of which waited for: 3 -> 5; matrix products, arithmetic and copies ran while one was open for 6% -> 5% of each run, Pallas kernels for 0% -> 0%
where the time goes in v1:
time: 522 us
  waiting for transfers between devices  411 us (79%)
  matrix products  42.5 us (8%)
  local copies, waits for them, and re-layouts  40.4 us (8%)
  between operations  14.1 us (3%)
  other arithmetic  10.3 us (2%)
    all_gather x1, waiting for transfers between devices, body(): lax.all_gather(up_local, 'fs', axis=0, tiled=True)  200 us
    all_gather x1, waiting for transfers between devices, body(): lax.all_gather(gate_local, 'fs', axis=0, tiled=True)  137 us
    ppermute x3, waiting for transfers between devices, plan_islands(): prior = plan_islands([lax.ppermute(seen_now[0], 'tp', sheets), *seen_now])  73.3 us
    unnamed x15, local copies, waits for them, and re-layouts  40.3 us
    dot_general x1, matrix products, body(): up_acc = jnp.dot(normed, up_serve, preferred_element_type=jnp.float32)  22 us
    dot_general x1, matrix products, body(): gate_acc = jnp.dot(normed, gate_serve, preferred_element_type=jnp.float32)  20.5 us
  transfers between devices with their start and end apart: 5, of which 5 were waited for; matrix products, arithmetic and copies ran while one was open for 5% of the time, Pallas kernels for 0%

profile of v1, /device:TPU:0, one launch (start us, length us, event | category | flops | bytes accessed | tf_op | source)
XLA Modules:
  0.0 522.2 jit_solution(16411072097817935836)
XLA Ops:
  7.2 0.0 copy-start.1
  7.2 0.0 all-gather.3.cloned.1.call-start
  7.2 9.4 %multiply_convert_fusion.1 = (bf16[512,3072]{1,0:T(8,128)(2,1)}, bf16[512,3072]{1,0:T(8,128)(2,1)}) fusion(f32[512,3072]{1,0:T(8,128)} %param.7, f32[512]{0:T(512)} %param.5, f32[512,3072]{1,0:T(8,128)} %param.6), kind=kLoop, calls=%fused_computation.5 | loop fusion | flops 6291456 | bytes 18876416 | tf_op jit(solution)/shard_map/convert_element_type | solution.py:26
  16.6 0.0 all-gather.3.cloned.1.call-update
  16.6 0.0 all-gather.5.cloned.1.call-start
  16.7 0.7 all-gather.5.cloned.1.call-update
  17.4 0.0 copy-done.1
  17.4 3.0 collective-permute-start
  20.4 24.1 %collective-permute-done = bf16[512,1024]{1,0:T(8,128)(2,1)S(1)} collective-permute-done((bf16[512,1024]{1,0:T(8,128)(2,1)S(1)}, bf16[512,1024]{1,0:T(8,128)(2,1)S(1)}, u32[]{:S(2)}, u32[]{:S(2)}) %collective-permute-start) | collective-permute-done | bytes 1048608 | tf_op jit(solution)/shard_map/ppermute | solution.py:14
  44.5 0.8 collective-permute-start.1
  45.3 24.5 %collective-permute-done.1 = bf16[512,1024]{1,0:T(8,128)(2,1)S(1)} collective-permute-done((bf16[512,1024]{1,0:T(8,128)(2,1)S(1)}, bf16[512,1024]{1,0:T(8,128)(2,1)S(1)}, u32[]{:S(2)}, u32[]{:S(2)}) %collective-permute-start.1) | collective-permute-done | bytes 1048608 | tf_op jit(solution)/shard_map/ppermute | solution.py:14
  69.8 0.0 collective-permute-start.2
  69.8 24.7 %collective-permute-done.2 = bf16[512,1024]{1,0:T(8,128)(2,1)} collective-permute-done((bf16[512,1024]{1,0:T(8,128)(2,1)S(1)}, bf16[512,1024]{1,0:T(8,128)(2,1)}, u32[]{:S(2)}, u32[]{:S(2)}) %collective-permute-start.2) | collective-permute-done | bytes 1048608 | tf_op jit(solution)/shard_map/ppermute | solution.py:14
  94.5 1.3 constant_dynamic-update-slice_fusion.7
  95.8 0.1 constant_dynamic-update-slice_fusion.6
  95.9 0.1 constant_dynamic-update-slice_fusion.5
  96.0 0.1 constant_dynamic-update-slice_fusion.4
  96.1 1.3 constant_dynamic-update-slice_fusion.3
  97.5 0.1 constant_dynamic-update-slice_fusion.2
  97.6 0.1 constant_dynamic-update-slice_fusion.1
  97.6 0.1 constant_dynamic-update-slice_fusion
  97.7 0.0 copy-start.2
  97.8 3.4 copy-done.2
  101.1 0.9 fusion
  102.0 137.3 %all-gather.3.cloned.1.call-done = bf16[4096,3072]{1,0:T(8,128)(2,1)} async-done(((bf16[512,3072]{1,0:T(8,128)(2,1)}), bf16[4096,3072]{1,0:T(8,128)(2,1)}) %all-gather.3.cloned.1.call-update) | async-done | bytes 25165840 | tf_op jit(solution)/shard_map/all_gather | solution.py:35
  239.3 20.5 %fusion.3 = f32[512,3072]{1,0:T(8,128)} fusion(bf16[4096,3072]{1,0:T(8,128)(2,1)} %all-gather.3.cloned.1.call-done, f32[512]{0:T(512)S(1)} %add_rsqrt_fusion, bf16[512,8192]{1,0:T(8,128)(2,1)} %copy-done.2, s32[]{:T(128)S(6)} %select_n.14), kind=kOutput, calls=%fused_computation.7 | convolution fusion | flops 12891193344 | bytes 35653636 | tf_op jit(solution)/shard_map/dot_general | solution.py:38
  259.8 199.8 %all-gather.5.cloned.1.call-done = bf16[4096,3072]{1,0:T(8,128)(2,1)} async-done(((bf16[512,3072]{1,0:T(8,128)(2,1)}), bf16[4096,3072]{1,0:T(8,128)(2,1)}) %all-gather.5.cloned.1.call-update) | async-done | bytes 25165840 | tf_op jit(solution)/shard_map/all_gather | solution.py:36
  459.6 22.0 %multiply_convert_fusion = bf16[512,3072]{1,0:T(8,128)(2,1)} fusion(f32[512,3072]{1,0:T(8,128)} %fusion.3, bf16[4096,3072]{1,0:T(8,128)(2,1)} %all-gather.5.cloned.1.call-done, f32[512]{0:T(512)S(1)} %add_rsqrt_fusion, bf16[512,8192]{1,0:T(8,128)(2,1)} %copy-done.2, s32[]{:T(128)S(6)} %select_n.14), kind=kOutput, calls=%fused_computation.4 | convolution fusion | flops 12903776256 | bytes 38799364 | tf_op jit(solution)/shard_map/dot_general | solution.py:39
  481.6 0.0 copy-start
  481.6 22.0 %copy.16 = bf16[4096,3072]{1,0:T(8,128)(2,1)} copy(bf16[4096,3072]{1,0:T(8,128)(2,1)} %all-gather.3.cloned.1.call-done) | data formatting | bytes 50331648
  503.5 2.9 copy-done
  506.5 8.9 %copy.17 = bf16[4096,3072]{1,0:T(8,128)(2,1)} copy(bf16[4096,3072]{1,0:T(8,128)(2,1)S(1)} %copy-done) | data formatting | bytes 50331648
  (1 shorter events, 0.0 us)
Async XLA Ops:
  7.2 10.2 %copy-start.1 = (bf16[512,1024]{1,0:T(8,128)(2,1)S(1)}, bf16[512,1024]{1,0:T(8,128)(2,1)}, u32[]{:S(2)}) copy-start(bf16[512,1024]{1,0:T(8,128)(2,1)} %param.4) | copy-start | bytes 3145732
  7.2 232.2 %all-gather.3.cloned.1.call-start = ((), (), s32[]{:S(2)}) async-start(), calls=%async_computation | async-start | bytes 28311552 | tf_op jit(solution)/shard_map/all_gather | solution.py:35
  16.6 443.0 %all-gather.5.cloned.1.call-start = ((), (), s32[]{:S(2)}) async-start(), calls=%async_computation.1 | async-start | bytes 28311552 | tf_op jit(solution)/shard_map/all_gather | solution.py:36
  17.4 27.1 %collective-permute-start = (bf16[512,1024]{1,0:T(8,128)(2,1)S(1)}, bf16[512,1024]{1,0:T(8,128)(2,1)S(1)}, u32[]{:S(2)}, u32[]{:S(2)}) collective-permute-start(bf16[512,1024]{1,0:T(8,128)(2,1)S(1)} %copy-done.1), channel_id=1, source_target_pairs={{0,1},{1,2},{2,3},{3,0},{4,5},{5,6},{6,7},{7,4},{8,9},{9,10},{10,1... | collective-permute-start | bytes 3145736 | tf_op jit(solution)/shard_map/ppermute | solution.py:14
  44.5 25.3 %collective-permute-start.1 = (bf16[512,1024]{1,0:T(8,128)(2,1)S(1)}, bf16[512,1024]{1,0:T(8,128)(2,1)S(1)}, u32[]{:S(2)}, u32[]{:S(2)}) collective-permute-start(bf16[512,1024]{1,0:T(8,128)(2,1)S(1)} %collective-permute-done), channel_id=1, source_target_pairs={{0,1},{1,2},{2,3},{3,0},{4,5},{5,6},{6,7},{7,4},{8,9},{9,10},{10,1... | collective-permute-start | bytes 3145736 | tf_op jit(solution)/shard_map/ppermute | solution.py:14
  69.8 24.7 %collective-permute-start.2 = (bf16[512,1024]{1,0:T(8,128)(2,1)S(1)}, bf16[512,1024]{1,0:T(8,128)(2,1)}, u32[]{:S(2)}, u32[]{:S(2)}) collective-permute-start(bf16[512,1024]{1,0:T(8,128)(2,1)S(1)} %collective-permute-done.1), channel_id=1, source_target_pairs={{0,1},{1,2},{2,3},{3,0},{4,5},{5,6},{6,7},{7,4},{8,9},{9,10},{10,1... | collective-permute-start | bytes 3145736 | tf_op jit(solution)/shard_map/ppermute | solution.py:14
  97.7 3.4 copy-start.2
  481.6 24.9 %copy-start = (bf16[4096,3072]{1,0:T(8,128)(2,1)S(1)}, bf16[4096,3072]{1,0:T(8,128)(2,1)}, u32[]{:S(2)}) copy-start(bf16[4096,3072]{1,0:T(8,128)(2,1)} %all-gather.5.cloned.1.call-done) | copy-start | bytes 75497472
Sparse Core Ops, SparseCore 0:
  16.7 222.5 all-gather.2
  241.5 218.0 all-gather.4
